TPU v7x, 32 devices: a whole 2x2x4 slice. The times are simulated.
32 devices in a mesh: ep: 4 (over y, x), tp: 8 (over z, core).
Axes of the slice: x: 2, y: 2, z: 4, core: 2. Of those that a mesh axis runs over, the one named last changes fastest.
Arguments:
- tokens: bfloat16 [768, 2048], P('ep'), may hold values from -6 to 6
- cotangent: bfloat16 [768, 2048], P('ep'), may hold values from -6 to 6
- routing: int32 [768, 2], P('ep'), may hold values from 0 to 3, all different within a row; in each aligned block of 192 rows (0 to 191, 192 to 383, ...) at most 192 rows name the same one
- gate_weights: bfloat16 [768, 2], P('ep'), may hold values from 0.19921875 to 1
- gate_proj: bfloat16 [4, 2048, 7168], P('ep', None, 'tp'), may hold values from -0.125 to 0.125
- up_proj: bfloat16 [4, 2048, 7168], P('ep', None, 'tp'), may hold values from -0.125 to 0.125
- down_proj: bfloat16 [4, 7168, 2048], P('ep', 'tp'), may hold values from -0.0625 to 0.0625
Outputs:
- grad_tokens: bfloat16 [768, 2048], P('ep', 'tp')
- grad_gates: float32 [768, 2], P('ep')
- grad_gate_proj: bfloat16 [4, 2048, 7168], P('ep', None, 'tp')
- grad_up_proj: bfloat16 [4, 2048, 7168], P('ep', None, 'tp')
- grad_down_proj: bfloat16 [4, 7168, 2048], P('ep', 'tp')
Inputs may be any that keep to these rules, and one draw needn't show every extreme that they name: `routing`: each row names 2 different experts. Within each aligned block of 192 rows no expert is named by more than 192 rows, and in every draw some expert is named by exactly 192 rows of some block.
All inputs are finite; a program needn't handle non-finite values.
Results may differ from a plain program's by a relative error of at most 0.019.
Values may be sent and summed in bfloat16 or wider, within the bound.
A program may use at most 128 MiB of HBM per device.

v0:
```python
import jax
import jax.numpy as jnp
from jax import lax
from jax.sharding import PartitionSpec as P


def expert_backward(in_rows, cot_rows, gate_col, w_gate, w_up, w_down):
    gate_pre = jnp.dot(in_rows, w_gate, preferred_element_type=jnp.float32)
    up_value = jnp.dot(in_rows, w_up, preferred_element_type=jnp.float32)
    sigmoid_val = jax.nn.sigmoid(gate_pre)
    active = gate_pre * sigmoid_val
    hidden = (active * up_value).astype(jnp.bfloat16)
    contract_cols = (((1,), (1,)), ((), ()))
    contract_rows = (((0,), (0,)), ((), ()))
    back_hidden = lax.dot_general(
        cot_rows, w_down, contract_cols, preferred_element_type=jnp.float32
    )
    gate_part = jnp.sum(hidden.astype(jnp.float32) * back_hidden, axis=1)
    scaled_back = gate_col * back_hidden
    grad_pre = (
        scaled_back * up_value * sigmoid_val * (1.0 + gate_pre * (1.0 - sigmoid_val))
    ).astype(jnp.bfloat16)
    grad_upval = (scaled_back * active).astype(jnp.bfloat16)
    scaled_cot = (gate_col * cot_rows.astype(jnp.float32)).astype(jnp.bfloat16)
    grad_down = lax.dot_general(
        hidden, scaled_cot, contract_rows, preferred_element_type=jnp.float32
    ).astype(jnp.bfloat16)
    grad_gate = lax.dot_general(
        in_rows, grad_pre, contract_rows, preferred_element_type=jnp.float32
    ).astype(jnp.bfloat16)
    grad_upw = lax.dot_general(
        in_rows, grad_upval, contract_rows, preferred_element_type=jnp.float32
    ).astype(jnp.bfloat16)
    grad_in = lax.dot_general(grad_pre, w_gate, contract_cols, preferred_element_type=jnp.float32)
    grad_in = grad_in + lax.dot_general(
        grad_upval, w_up, contract_cols, preferred_element_type=jnp.float32
    )
    return (grad_in, gate_part, grad_gate, grad_upw, grad_down)


def local(tokens, cotangent, routing, gate_weights, gate_proj, up_proj, down_proj):
    expert_count = lax.axis_size("ep")
    tok_rows, model_width = tokens.shape
    top_k = routing.shape[1]
    capacity = 2 * tok_rows * top_k // expert_count
    flat_routes = routing.reshape(-1)
    onehot = (flat_routes[:, None] == jnp.arange(expert_count, dtype=jnp.int32)[None, :]).astype(
        jnp.int32
    )
    position = jnp.sum(jnp.cumsum(onehot, axis=0) * onehot, axis=1) - 1
    slot_index = flat_routes * capacity + position
    slot_owner = (
        jnp.full((expert_count * capacity,), -1, jnp.int32)
        .at[slot_index]
        .set(jnp.arange(flat_routes.shape[0], dtype=jnp.int32))
    )
    is_used = slot_owner >= 0
    safe_owner = jnp.where(is_used, slot_owner, 0)
    token_index = safe_owner // top_k
    slot_gates = jnp.where(
        is_used, gate_weights.reshape(-1)[safe_owner], jnp.zeros((), jnp.bfloat16)
    )
    slot_gates = slot_gates.reshape(expert_count, capacity)

    def gather_slots(source):
        picked_rows = jnp.where(is_used[:, None], source[token_index], jnp.zeros((), jnp.bfloat16))
        return picked_rows.reshape(expert_count, capacity, source.shape[1])

    col_width = model_width // lax.axis_size("tp")
    col_start = lax.axis_index("tp") * col_width
    token_cols = lax.dynamic_slice_in_dim(tokens, col_start, col_width, 1)
    cot_cols = lax.dynamic_slice_in_dim(cotangent, col_start, col_width, 1)
    rows_part, cots_part, gates_in = (
        lax.all_to_all(gather_slots(token_cols), "ep", split_axis=0, concat_axis=0, tiled=True),
        lax.all_to_all(gather_slots(cot_cols), "ep", split_axis=0, concat_axis=0, tiled=True),
        lax.all_to_all(slot_gates, "ep", split_axis=0, concat_axis=0, tiled=True),
    )
    in_rows, cot_in = (
        lax.all_gather(rows_part, "tp", axis=2, tiled=True),
        lax.all_gather(cots_part, "tp", axis=2, tiled=True),
    )
    slot_count = in_rows.shape[0] * in_rows.shape[1]
    grad_in, gate_part, grad_gate, grad_upw, grad_down = expert_backward(
        in_rows.reshape(slot_count, model_width),
        cot_in.reshape(slot_count, model_width),
        gates_in.reshape(slot_count, 1).astype(jnp.float32),
        gate_proj[0],
        up_proj[0],
        down_proj[0],
    )
    gate_total = lax.psum(gate_part, "tp")
    grad_cols = lax.psum_scatter(
        grad_in.astype(jnp.bfloat16), "tp", scatter_dimension=1, tiled=True
    ).astype(jnp.float32)
    back_rows, back_gates = (
        lax.all_to_all(
            grad_cols.reshape(expert_count, capacity, grad_cols.shape[1]).astype(jnp.bfloat16),
            "ep",
            split_axis=0,
            concat_axis=0,
            tiled=True,
        ).astype(jnp.float32),
        lax.all_to_all(
            gate_total.reshape(expert_count, capacity).astype(jnp.bfloat16),
            "ep",
            split_axis=0,
            concat_axis=0,
            tiled=True,
        ).astype(jnp.float32),
    )
    picked = back_rows.reshape(expert_count * capacity, back_rows.shape[2])[slot_index]
    grad_tokens = jnp.sum(picked.reshape(tok_rows, top_k, picked.shape[1]), axis=1).astype(
        jnp.bfloat16
    )
    grad_gates = back_gates.reshape(-1)[slot_index].reshape(tok_rows, top_k)
    return (grad_tokens, grad_gates, grad_gate[None], grad_upw[None], grad_down[None])


def solution(mesh):
    return jax.shard_map(
        local,
        mesh=mesh,
        in_specs=(
            P("ep", None),
            P("ep", None),
            P("ep", None),
            P("ep", None),
            P("ep", None, "tp"),
            P("ep", None, "tp"),
            P("ep", "tp", None),
        ),
        out_specs=(
            P("ep", "tp"),
            P("ep", None),
            P("ep", None, "tp"),
            P("ep", None, "tp"),
            P("ep", "tp", None),
        ),
        check_vma=False,
    )
```

profile of v0, /device:TPU:0, one launch (start us, length us, event | category | flops | bytes accessed | tf_op | source)
XLA Modules:
  0.0 190.2 jit_solution(14403034976079991736)
XLA Ops:
  7.2 0.8 copy.18
  8.0 0.1 eq.29
  8.2 0.1 eq.25
  8.3 0.7 broadcast_multiply_fusion
  9.0 1.2 reduce-window.6
  10.2 0.2 slice_reduce_fusion
  10.4 0.2 reduce-window.9
  10.6 0.1 add_bitcast_fusion
  10.7 0.1 copy.17
  10.8 0.1 mul.64
  11.0 2.9 %scatter_custom_fusion = s32[768]{0:T(1024)S(1)} fusion(s32[384]{0:T(512)S(1)} %fusion.21, s32[384]{0:T(512)S(1)} %iota.11, s32[]{:T(128)} %constant.13.clone.1), kind=kCustom, calls=%fused_computation.55 | custom fusion | bytes 3076 | tf_op jit(solution)/shard_map/scatter | solution.py:55
  14.0 0.1 broadcast_in_dim.52
  14.1 1.0 constant_dynamic-slice_fusion
  15.0 2.7 %gather_fusion.2 = bf16[768,256]{1,0:T(8,128)(2,1)S(1)} fusion(bf16[192,256]{1,0:T(8,128)(2,1)S(1)} %get-tuple-element.23, s32[1024]{0:T(1024)S(1)} %pad_clamp_fusion.1), kind=kCustom, calls=%fused_computation.2 | custom fusion | bytes 789504 | tf_op jit(solution)/shard_map/gather | solution.py:66
  17.7 2.7 %gather_fusion.1 = bf16[768,256]{1,0:T(8,128)(2,1)S(1)} fusion(bf16[192,256]{1,0:T(8,128)(2,1)S(1)} %get-tuple-element.24, s32[1024]{0:T(1024)S(1)} %pad_clamp_fusion.1), kind=kCustom, calls=%fused_computation.1 | custom fusion | bytes 789504 | tf_op jit(solution)/shard_map/gather | solution.py:66
  20.4 0.2 broadcast_select_fusion.1
  20.5 12.2 %all_to_all.31 = bf16[4,192,256]{2,1,0:T(8,128)(2,1)} all-to-all(bf16[4,192,256]{2,1,0:T(8,128)(2,1)S(1)} %get-tuple-element.22), channel_id=1, replica_groups=mesh['ep'=4,'tp'=8] {'ep'}, dimensions={0} | all-to-all | bytes 786432 | tf_op jit(solution)/shard_map/all_to_all | solution.py:74
  32.8 9.5 %all_to_all.32 = bf16[4,192,256]{2,1,0:T(8,128)(2,1)} all-to-all(bf16[4,192,256]{2,1,0:T(8,128)(2,1)S(1)} %get-tuple-element.21), channel_id=1, replica_groups=mesh['ep'=4,'tp'=8] {'ep'}, dimensions={0} | all-to-all | bytes 786432 | tf_op jit(solution)/shard_map/all_to_all | solution.py:75
  42.4 0.0 reduce-scatter.2.cloned.1.call-start
  42.4 0.1 copy.20
  42.6 0.2 reshape.132
  42.7 5.0 %gather_fusion = bf16[768]{0:T(1024)(128)(2,1)S(1)} fusion(bf16[384]{0:T(512)(128)(2,1)S(1)} %reshape.132, s32[1024]{0:T(1024)S(1)} %pad_clamp_fusion.2), kind=kCustom, calls=%fused_computation | custom fusion | bytes 6144 | tf_op jit(solution)/shard_map/gather | solution.py:61
  47.8 0.1 all_to_all.25
  47.9 7.0 %all_to_all.33 = bf16[4,1,192]{2,1,0:T(2,128)(2,1)S(1)} all-to-all(bf16[4,1,192]{2,1,0:T(2,128)(2,1)S(1)} %all_to_all.25), channel_id=1, replica_groups=mesh['ep'=4,'tp'=8] {'ep'}, dimensions={0} | all-to-all | bytes 3072 | tf_op jit(solution)/shard_map/all_to_all | solution.py:76
  54.9 0.1 reshape.139
  55.0 16.9 %all-gather.5.cloned.1.call-done = bf16[4,192,2048]{2,1,0:T(8,128)(2,1)} async-done(((bf16[4,192,256]{2,1,0:T(8,128)(2,1)}), bf16[4,192,2048]{2,1,0:T(8,128)(2,1)}) %all-gather.5.cloned.1.call-update) | async-done | bytes 3145744 | tf_op jit(solution)/shard_map/all_gather | solution.py:79
  71.8 8.1 %fusion.2 = f32[768,896]{1,0:T(8,128)} fusion(bf16[768,2048]{1,0:T(8,128)(2,1)} %bitcast.60, bf16[1,2048,896]{2,1,0:T(8,128)(2,1)} %param.11), kind=kOutput, calls=%fused_computation.10 | convolution fusion | flops 2818572288 | bytes 9568256 | tf_op jit(solution)/shard_map/dot_general | solution.py:8
  79.9 5.0 %fusion.6 = f32[768,896]{1,0:T(8,128)} fusion(bf16[768,2048]{1,0:T(8,128)(2,1)S(1)} %bitcast.61, bf16[1,2048,896]{2,1,0:T(8,128)(2,1)S(1)} %copy-done.2), kind=kOutput, calls=%fused_computation.14 | convolution fusion | flops 2818572288 | bytes 9568256 | tf_op jit(solution)/shard_map/dot_general | solution.py:9
  84.9 26.0 %all-gather.3.cloned.1.call-done = bf16[4,192,2048]{2,1,0:T(8,128)(2,1)} async-done(((bf16[4,192,256]{2,1,0:T(8,128)(2,1)}), bf16[4,192,2048]{2,1,0:T(8,128)(2,1)}) %all-gather.3.cloned.1.call-update) | async-done | bytes 3145744 | tf_op jit(solution)/shard_map/all_gather | solution.py:80
  110.8 9.9 %multiply_reduce_fusion = (f32[768]{0:T(1024)S(1)}, bf16[768,896]{1,0:T(8,128)(2,1)}, bf16[768,896]{1,0:T(8,128)(2,1)S(1)}, bf16[768,896]{1,0:T(8,128)(2,1)S(1)}) fusion(f32[768,896]{1,0:T(8,128)} %fusion.6, f32[768,896]{1,0:T(8,128)} %fusion.2, f32[768]{0:T(1024)S(1)} %reshape.139, bf16[768,2048]{1,0:T(8,128)(2,1)} %bitcast.64, ...), kind=kOutput, calls=%fused_computation.22 | convolution fusion | flops 2831645952 | bytes 16455680 | tf_op jit(solution)/shard_map/dot_general | solution.py:15
  120.7 3.4 %fusion = f32[768,2048]{1,0:T(8,128)S(1)} fusion(bf16[768,896]{1,0:T(8,128)(2,1)S(1)} %get-tuple-element.19, bf16[1,2048,896]{2,1,0:T(8,128)(2,1)S(1)} %copy-done.1), kind=kOutput, calls=%fused_computation.8 | convolution fusion | flops 2818572288 | bytes 11337728 | tf_op jit(solution)/shard_map/dot_general | solution.py:34
  124.2 4.8 %add_convert_fusion = bf16[768,2048]{1,0:T(8,128)(2,1)} fusion(f32[768,2048]{1,0:T(8,128)S(1)} %fusion, bf16[768,896]{1,0:T(8,128)(2,1)S(1)} %get-tuple-element.20, bf16[1,2048,896]{2,1,0:T(8,128)(2,1)S(1)} %copy-done.3), kind=kOutput, calls=%fused_computation.7 | convolution fusion | flops 2821718016 | bytes 14483456 | tf_op jit(solution)/shard_map/dot_general | solution.py:35
  129.1 15.3 %psum.7 = bf16[768]{0:T(1024)(128)(2,1)S(1)} all-reduce(f32[768]{0:T(1024)S(1)} %get-tuple-element.15), channel_id=1, replica_groups=mesh['ep'=4,'tp'=8] {'tp'}, use_global_device_ids=true, to_apply=%region_7.8 | all-reduce | flops 768 | bytes 4608 | tf_op jit(solution)/shard_map/psum | solution.py:91
  144.4 0.7 convert_element_type.96
  145.1 3.5 %all-to-all-start.4 = ((bf16[4,1,192]{2,1,0:T(2,128)(2,1)}), bf16[4,1,192]{2,1,0:T(2,128)(2,1)S(1)}, u32[]{:S(2)}, u32[]{:S(2)}) async-start(bf16[4,1,192]{2,1,0:T(2,128)(2,1)} %convert_element_type.96), calls=%async_computation.5 | async-start | bytes 8192 | tf_op jit(solution)/shard_map/all_to_all | solution.py:103
  148.6 7.5 %convert_bitcast_fusion = bf16[1,896,2048]{2,1,0:T(8,128)(2,1)} fusion(bf16[768,896]{1,0:T(8,128)(2,1)} %get-tuple-element.16, bf16[768,2048]{1,0:T(8,128)(2,1)} %bitcast.65, f32[768]{0:T(1024)S(1)} %reshape.139), kind=kOutput, calls=%fused_computation.18 | convolution fusion | flops 2825125888 | bytes 8195072 | tf_op jit(solution)/shard_map/dot_general | solution.py:25
  156.0 5.0 %convert_bitcast_fusion.1 = bf16[1,2048,896]{2,1,0:T(8,128)(2,1)} fusion(bf16[768,2048]{1,0:T(8,128)(2,1)S(1)} %bitcast.62, bf16[768,896]{1,0:T(8,128)(2,1)S(1)} %copy-done.7), kind=kOutput, calls=%fused_computation.19 | convolution fusion | flops 2820407296 | bytes 8192000 | tf_op jit(solution)/shard_map/dot_general | solution.py:31
  161.0 7.0 %reduce-scatter.2.cloned.1.call-done = bf16[768,256]{1,0:T(8,128)(2,1)} async-done(((bf16[768,2048]{1,0:T(8,128)(2,1)}), bf16[768,256]{1,0:T(8,128)(2,1)}) %reduce-scatter.2.cloned.1.call-update) | async-done | bytes 393232 | tf_op jit(solution)/shard_map/reduce_scatter | solution.py:92
  168.0 3.5 %all-to-all-start.3 = ((bf16[4,192,256]{2,1,0:T(8,128)(2,1)}), bf16[4,192,256]{2,1,0:T(8,128)(2,1)S(1)}, u32[]{:S(2)}, u32[]{:S(2)}) async-start(bf16[4,192,256]{2,1,0:T(8,128)(2,1)} %bitcast.58), calls=%async_computation.4 | async-start | bytes 786432 | tf_op jit(solution)/shard_map/all_to_all | solution.py:96
  171.5 6.3 %convert_bitcast_fusion.2 = bf16[1,2048,896]{2,1,0:T(8,128)(2,1)} fusion(bf16[768,2048]{1,0:T(8,128)(2,1)S(1)} %bitcast.63, bf16[768,896]{1,0:T(8,128)(2,1)} %copy-done.5), kind=kOutput, calls=%fused_computation.20 | convolution fusion | flops 2820407296 | bytes 8192000 | tf_op jit(solution)/shard_map/dot_general | solution.py:28
  177.8 0.1 reshape.142
  177.9 1.9 gather_fusion.4
  179.8 0.1 reshape.138
  179.9 0.7 copy.23
  180.6 0.1 bitcast_convert_fusion
  180.7 1.7 gather_fusion.3
  182.3 0.2 reshape.137
  182.6 1.1 reduce_sum.28
  (36 shorter events, 0.3 us)
Async XLA Ops:
  7.2 64.7 %all-gather.5.cloned.1.call-start = ((), (), s32[]{:S(2)}) async-start(), calls=%async_computation.7 | async-start | bytes 3538944 | tf_op jit(solution)/shard_map/all_gather | solution.py:79
  17.7 24.7 %copy-start = (bf16[192,2]{0,1:T(2,128)(2,1)S(1)}, bf16[192,2]{0,1:T(2,128)(2,1)}, u32[]{:S(2)}) copy-start(bf16[192,2]{0,1:T(2,128)(2,1)} %param.10) | copy-start | bytes 2308
  32.8 78.0 %all-gather.3.cloned.1.call-start = ((), (), s32[]{:S(2)}) async-start(), calls=%async_computation.6 | async-start | bytes 3538944 | tf_op jit(solution)/shard_map/all_gather | solution.py:80
  42.4 125.6 %reduce-scatter.2.cloned.1.call-start = ((), (), s32[]{:S(2)}) async-start(), calls=%async_computation.8 | async-start | bytes 3538944 | tf_op jit(solution)/shard_map/reduce_scatter | solution.py:92
  71.8 8.1 %copy-start.2 = (bf16[1,2048,896]{2,1,0:T(8,128)(2,1)S(1)}, bf16[1,2048,896]{2,1,0:T(8,128)(2,1)}, u32[]{:S(2)}) copy-start(bf16[1,2048,896]{2,1,0:T(8,128)(2,1)} %param.12) | copy-start | bytes 11010052
  71.8 8.1 %copy-start.4 = (bf16[4,192,2048]{2,1,0:T(8,128)(2,1)S(1)}, bf16[4,192,2048]{2,1,0:T(8,128)(2,1)}, u32[]{:S(2)}) copy-start(bf16[4,192,2048]{2,1,0:T(8,128)(2,1)} %all-gather.5.cloned.1.call-done) | copy-start | bytes 9437188
  110.8 9.9 %copy-start.1 = (bf16[1,2048,896]{2,1,0:T(8,128)(2,1)S(1)}, bf16[1,2048,896]{2,1,0:T(8,128)(2,1)}, u32[]{:S(2)}) copy-start(bf16[1,2048,896]{2,1,0:T(8,128)(2,1)} %param.11) | copy-start | bytes 11010052
  120.7 3.5 %copy-start.5 = (bf16[768,896]{1,0:T(8,128)(2,1)}, bf16[768,896]{1,0:T(8,128)(2,1)S(1)}, u32[]{:S(2)}) copy-start(bf16[768,896]{1,0:T(8,128)(2,1)S(1)} %get-tuple-element.19) | copy-start | bytes 4128772
  120.7 3.5 %copy-start.6 = (bf16[768,896]{1,0:T(8,128)(2,1)}, bf16[768,896]{1,0:T(8,128)(2,1)S(1)}, u32[]{:S(2)}) copy-start(bf16[768,896]{1,0:T(8,128)(2,1)S(1)} %get-tuple-element.20) | copy-start | bytes 4128772
  120.7 3.5 %copy-start.3 = (bf16[1,2048,896]{2,1,0:T(8,128)(2,1)S(1)}, bf16[1,2048,896]{2,1,0:T(8,128)(2,1)}, u32[]{:S(2)}) copy-start(bf16[1,2048,896]{2,1,0:T(8,128)(2,1)} %param.12) | copy-start | bytes 11010052
  145.1 15.9 %all-to-all-start.4 = ((bf16[4,1,192]{2,1,0:T(2,128)(2,1)}), bf16[4,1,192]{2,1,0:T(2,128)(2,1)S(1)}, u32[]{:S(2)}, u32[]{:S(2)}) async-start(bf16[4,1,192]{2,1,0:T(2,128)(2,1)} %convert_element_type.96), calls=%async_computation.5 | async-start | bytes 8192 | tf_op jit(solution)/shard_map/all_to_all | solution.py:103
  148.6 7.5 %copy-start.7 = (bf16[768,896]{1,0:T(8,128)(2,1)S(1)}, bf16[768,896]{1,0:T(8,128)(2,1)}, u32[]{:S(2)}) copy-start(bf16[768,896]{1,0:T(8,128)(2,1)} %copy-done.6) | copy-start | bytes 4128772
  168.0 12.6 %all-to-all-start.3 = ((bf16[4,192,256]{2,1,0:T(8,128)(2,1)}), bf16[4,192,256]{2,1,0:T(8,128)(2,1)S(1)}, u32[]{:S(2)}, u32[]{:S(2)}) async-start(bf16[4,192,256]{2,1,0:T(8,128)(2,1)} %bitcast.58), calls=%async_computation.4 | async-start | bytes 786432 | tf_op jit(solution)/shard_map/all_to_all | solution.py:96
Sparse Core Ops, SparseCore 0:
  32.9 38.8 all-gather.4
  73.4 37.3 all-gather.2
  129.2 38.7 reduce-scatter.1
where the time goes:
time: 191 us; the launch traced here: 190 us
  waiting for transfers between devices  49.9 us (26%)
  matrix products  49.9 us (26%)
  blocking collectives  44.1 us (23%)
  local copies, waits for them, and re-layouts  21.7 us (11%)
  between operations  14 us (7%)
  starting transfers between devices  7.05 us (4%)
  other arithmetic  3.67 us (2%)
    all_gather x1, waiting for transfers between devices, local(): lax.all_gather(cots_part, 'tp', axis=2, tiled=True)  26 us
    all_gather x1, waiting for transfers between devices, local(): lax.all_gather(rows_part, 'tp', axis=2, tiled=True)  16.9 us
    psum x1, blocking collectives, local(): gate_total = lax.psum(gate_part, 'tp')  15.3 us
    all_to_all x1, blocking collectives, local(): lax.all_to_all(gather_slots(token_cols), 'ep', split_axis=0, concat_axis=...  12.2 us
    dot_general x1, matrix products, expert_backward(): lax.dot_general(cot_rows, w_down, contract_cols, preferred_element_type=j...  9.88 us
    all_to_all x1, blocking collectives, local(): lax.all_to_all(gather_slots(cot_cols), 'ep', split_axis=0, concat_axis=0,...  9.5 us
    dot_general x1, matrix products, expert_backward(): gate_pre = jnp.dot(in_rows, w_gate, preferred_element_type=jnp.float32)  8.07 us
    dot_general x1, matrix products, expert_backward(): lax.dot_general(hidden, scaled_cot, contract_rows, preferred_element_type...  7.45 us
  transfers between devices with their start and end apart: 5, of which 3 were waited for; matrix products, arithmetic and copies ran while one was open for 21% of the time, Pallas kernels for 0%

commit v1 on v0

--- a/solution.py
+++ b/solution.py
@@ -1,6 +1,8 @@
 import jax
 import jax.numpy as jnp
 from jax import lax
+from jax.experimental import pallas as pl
+from jax.experimental.pallas import tpu as pltpu
 from jax.sharding import PartitionSpec as P
 
 
@@ -38,7 +40,7 @@
     return (grad_in, gate_part, grad_gate, grad_upw, grad_down)
 
 
-def local(tokens, cotangent, routing, gate_weights, gate_proj, up_proj, down_proj):
+def slotted(tokens, cotangent, routing, gate_weights, gate_proj, up_proj, down_proj):
     expert_count = lax.axis_size("ep")
     tok_rows, model_width = tokens.shape
     top_k = routing.shape[1]
@@ -116,6 +118,231 @@
     return (grad_tokens, grad_gates, grad_gate[None], grad_upw[None], grad_down[None])
 
 
+MESH = pl.DeviceIdType.MESH
+
+
+def flip(index, mask):
+    if mask & 1:
+        index = index + 1 - 2 * (index % 2)
+    if mask & 2:
+        index = index + 2 - 4 * ((index // 2) % 2)
+    if mask & 4:
+        index = index + 4 - 8 * ((index // 4) % 2)
+    return index
+
+
+class Copies:
+    def __init__(self, send_sem, recv_sem):
+        self.send_sem, self.recv_sem, self.made = send_sem, recv_sem, []
+
+    def send(self, src, dst, ep, tp):
+        n = len(self.made)
+        copy = pltpu.make_async_remote_copy(
+            src_ref=src,
+            dst_ref=dst,
+            send_sem=self.send_sem.at[n],
+            recv_sem=self.recv_sem.at[n],
+            device_id=(ep, tp),
+            device_id_type=MESH,
+        )
+        copy.start()
+        self.made.append(copy)
+        return copy
+
+    def finish(self):
+        for copy in self.made:
+            copy.wait_send()
+
+
+def gather_kernel(tok, cot, gate, tok_out, cot_out, gate_out, send_sem, recv_sem, own_sem):
+    me, t = lax.axis_index("ep"), lax.axis_index("tp")
+    width = tok.shape[1]
+    eighth = width // 8
+    quarter = 2 * eighth
+    q, far = t % 4, flip(t % 4, 2)
+
+    def cols(start, size):
+        return pl.ds(pl.multiple_of(start, 128), size)
+
+    low, high = cols(quarter * q, eighth), cols(quarter * q + eighth, eighth)
+    full = cols(quarter * q, quarter)
+    far_low, far_high = cols(quarter * far, eighth), cols(quarter * far + eighth, eighth)
+    far_full = cols(quarter * far, quarter)
+    pairs = ((tok, tok_out), (cot, cot_out))
+    own = [
+        pltpu.make_async_copy(src, dst.at[0], own_sem.at[a]) for a, (src, dst) in enumerate(pairs)
+    ]
+    for copy in own:
+        copy.start()
+    do = Copies(send_sem, recv_sem)
+    gates = [do.send(gate.at[j], gate_out.at[j], flip(me, j), t) for j in (1, 2, 3)]
+    relayed, direct = [], []
+    for src, dst in pairs:
+        for j, where in ((3, full), (1, high), (2, high)):
+            copy = do.send(src.at[:, where], dst.at[j, :, where], flip(me, j), t)
+            relayed.append((copy, dst, j, where))
+    for src, dst in pairs:
+        for where in (low, far_low):
+            for j in (1, 2):
+                copy = do.send(src.at[:, where], dst.at[j, :, where], flip(me, j), t)
+                direct.append((copy, dst, j, where))
+    last = []
+    for copy, dst, j, where in relayed:
+        copy.wait_recv()
+        piece = dst.at[j, :, where]
+        moved = do.send(piece, piece, me, flip(t, 2))
+        direct.append((moved, dst, j, far_full if j == 3 else far_high))
+        last.append(do.send(piece, piece, me, flip(t, 1)))
+    for copy, dst, j, where in direct:
+        copy.wait_recv()
+        piece = dst.at[j, :, where]
+        last.append(do.send(piece, piece, me, flip(t, 1)))
+    for copy in last + gates:
+        copy.wait_recv()
+    do.finish()
+    gate_out[0] = gate[0]
+    for copy in own:
+        copy.wait()
+
+
+def gather(tokens, cotangent, gate):
+    experts = lax.axis_size("ep")
+    shape = jax.ShapeDtypeStruct((experts,) + tokens.shape, tokens.dtype)
+    vmem = pl.BlockSpec(memory_space=pltpu.VMEM)
+    return pl.pallas_call(
+        gather_kernel,
+        out_shape=[shape, shape, jax.ShapeDtypeStruct(gate.shape, gate.dtype)],
+        in_specs=[vmem] * 3,
+        out_specs=[vmem] * 3,
+        scratch_shapes=[
+            pltpu.SemaphoreType.DMA((43,)),
+            pltpu.SemaphoreType.DMA((43,)),
+            pltpu.SemaphoreType.DMA((2,)),
+        ],
+        compiler_params=pltpu.CompilerParams(has_side_effects=True),
+    )(tokens, cotangent, gate)
+
+
+def reduce_kernel(part, gate, out, gate_out, r1, m, r2, s, r3, rg, g, send_sem, recv_sem):
+    me, t = lax.axis_index("ep"), lax.axis_index("tp")
+    core, z = t % 2, t // 2
+    size = out.shape[1]
+    other = flip(t, 1)
+    order = (3, 2, 1, 0)
+    blocks = (3, 1, 2, 0)
+    f32 = jnp.float32
+
+    def cols(d, which):
+        return pl.ds(pl.multiple_of((2 * flip(z, d) + which) * size, 128), size)
+
+    do = Copies(send_sem, recv_sem)
+    first = {}
+    for d in order:
+        for j in blocks:
+            first[d, j] = do.send(part.at[j, :, cols(d, 1 - core)], r1.at[d, j], me, other)
+        if d == 3:
+            stage = do.send(gate, rg.at[0], me, other)
+    second = {}
+    for n, d in enumerate(order):
+        for j in blocks:
+            first[d, j].wait_recv()
+            mine = part[j, :, cols(d, core)].astype(f32)
+            m[d, j] = (mine + r1[d, j].astype(f32)).astype(m.dtype)
+            if j > 0:
+                second[d, j] = do.send(m.at[d, j], r2.at[d, j], flip(me, j), t)
+        if n < 3:
+            stage.wait_recv()
+            g[n] = (gate[...] if n == 0 else g[n - 1]) + rg[n]
+            if n < 2:
+                stage = do.send(g.at[n], rg.at[n + 1], me, flip(t, 2 << n))
+    gates = [do.send(g.at[2, j], gate_out.at[j], flip(me, j), t) for j in (1, 2, 3)]
+    third = {}
+    for d in order:
+        total = m[d, 0].astype(f32)
+        for j in (1, 2, 3):
+            second[d, j].wait_recv()
+            total = total + r2[d, j].astype(f32)
+        if d:
+            s[d] = total.astype(s.dtype)
+            third[d] = do.send(s.at[d], r3.at[d], me, flip(t, 2 * d))
+    for d in (3, 2, 1):
+        third[d].wait_recv()
+        total = total + r3[d].astype(f32)
+    out[...] = total.astype(out.dtype)
+    for copy in gates:
+        copy.wait_recv()
+    do.finish()
+    gate_out[0] = g[2, 0]
+
+
+def reduce(part, gate):
+    experts, parts = lax.axis_size("ep"), lax.axis_size("tp")
+    rows, size = part.shape[1], part.shape[2] // parts
+    vmem = pl.BlockSpec(memory_space=pltpu.VMEM)
+    slots = parts // 2
+    tile = pltpu.VMEM((slots, experts, rows, size), part.dtype)
+    return pl.pallas_call(
+        reduce_kernel,
+        out_shape=[
+            jax.ShapeDtypeStruct((rows, size), part.dtype),
+            jax.ShapeDtypeStruct(gate.shape, gate.dtype),
+        ],
+        in_specs=[vmem] * 2,
+        out_specs=[vmem] * 2,
+        scratch_shapes=[
+            tile,
+            tile,
+            tile,
+            pltpu.VMEM((slots, rows, size), part.dtype),
+            pltpu.VMEM((slots, rows, size), part.dtype),
+            pltpu.VMEM((3,) + gate.shape, gate.dtype),
+            pltpu.VMEM((3,) + gate.shape, gate.dtype),
+            pltpu.SemaphoreType.DMA((37,)),
+            pltpu.SemaphoreType.DMA((37,)),
+        ],
+        compiler_params=pltpu.CompilerParams(has_side_effects=True),
+    )(part, gate)
+
+
+def tiles(values):
+    rows = values.shape[1]
+    padded = jnp.pad(values, ((0, 0), (0, -rows % 128)))
+    return jnp.broadcast_to(padded[:, None, :], (padded.shape[0], 8, padded.shape[1]))
+
+
+def dense(tokens, cotangent, routing, gate_weights, gate_proj, up_proj, down_proj):
+    f32, bf16 = jnp.float32, jnp.bfloat16
+    experts = lax.axis_size("ep")
+    rows, width = tokens.shape
+    me = lax.axis_index("ep")
+    named = [routing == (me ^ j) for j in range(experts)]
+    weights = jnp.stack(
+        [jnp.sum(jnp.where(n, gate_weights.astype(f32), 0.0), axis=1) for n in named]
+    )
+    x_all, cot_all, g_all = gather(tokens, cotangent, tiles(weights))
+    x, cot = x_all.reshape(-1, width), cot_all.reshape(-1, width)
+    g = g_all[:, 0, :rows].reshape(-1, 1)
+    grad_in, gate_part, d_gate, d_up, d_down = expert_backward(
+        x, cot, g, gate_proj[0], up_proj[0], down_proj[0]
+    )
+    grad_tokens, gate_sum = reduce(
+        grad_in.astype(bf16).reshape(experts, rows, width),
+        tiles(gate_part.reshape(experts, rows)),
+    )
+    grad_gates = jnp.zeros(routing.shape, f32)
+    for j in range(experts):
+        grad_gates = jnp.where(named[j], gate_sum[j, 0, :rows][:, None], grad_gates)
+    return grad_tokens, grad_gates, d_gate[None], d_up[None], d_down[None]
+
+
+def local(tokens, cotangent, routing, gate_weights, gate_proj, up_proj, down_proj):
+    experts, parts = lax.axis_size("ep"), lax.axis_size("tp")
+    capacity = 2 * tokens.shape[0] * routing.shape[1] // experts
+    fits = experts == 4 and parts == 8 and tokens.shape[1] % 1024 == 0
+    plan = dense if capacity >= tokens.shape[0] and fits else slotted
+    return plan(tokens, cotangent, routing, gate_weights, gate_proj, up_proj, down_proj)
+
+
 def solution(mesh):
     return jax.shard_map(
         local,

time: 191 us -> 122 us (0.64)
  Pallas kernels: 0 us -> 68.6 us
  waiting for transfers between devices: 49.9 us -> 0 us
  blocking collectives: 44.1 us -> 0 us
  local copies, waits for them, and re-layouts: 21.7 us -> 3.62 us
  between operations: 14 us -> 0.74 us
  starting transfers between devices: 7.05 us -> 0 us
  matrix products: 49.9 us -> 47.2 us
  other arithmetic: 3.67 us -> 1.32 us
    pallas_call x0 -> x2, Pallas kernels: none -> 68.6 us  [the longest x1 39.9 us: gather(): pl.pallas_call(gather_kernel, out_shape=[shape, shape, jax.ShapeDtypeStru...]
    all_gather x2 -> x0, waiting for transfers between devices: 42.8 us -> none  [the longest x1 26 us: local(): lax.all_gather(cots_part, 'tp', axis=2, tiled=True)]
    all_to_all x3 -> x0, blocking collectives: 28.7 us -> none  [the longest x1 12.2 us: local(): lax.all_to_all(gather_slots(token_cols), 'ep', split_axis=0, concat_axis=...]
    psum x1 -> x0, blocking collectives: 15.3 us -> none  [local(): gate_total = lax.psum(gate_part, 'tp')]
    gather x5 -> x0, local copies, waits for them, and re-layouts: 13.9 us -> none  [the longest x2 5.31 us: gather_slots(): source[token_index]]
    reduce_scatter x1 -> x0, waiting for transfers between devices: 6.99 us -> none  [local(): lax.psum_scatter(grad_in.astype(jnp.bfloat16), 'tp', scatter_dimension=1,...]
    all_to_all x2 -> x0, starting transfers between devices: 6.93 us -> none  [the longest x1 3.47 us: local(): lax.all_to_all(gate_total.reshape(expert_count, capacity).astype(jnp.bflo...]
    dot_general x1, matrix products: 8.07 us -> 4.94 us  [expert_backward(): gate_pre = jnp.dot(in_rows, w_gate, preferred_element_type=jnp.float32)]
  transfers between devices with their start and end apart: 5 -> 0, of which waited for: 3 -> 0; matrix products, arithmetic and copies ran while one was open for 21% -> 0% of each run, Pallas kernels for 0% -> 0%
where the time goes in v1:
time: 122 us; the launch traced here: 121 us
  Pallas kernels  68.6 us (56%)
  matrix products  47.2 us (39%)
  local copies, waits for them, and re-layouts  3.62 us (3%)
  other arithmetic  1.32 us (1%)
    pallas_call x1, Pallas kernels, gather(): pl.pallas_call(gather_kernel, out_shape=[shape, shape, jax.ShapeDtypeStru...  39.9 us
    pallas_call x1, Pallas kernels, reduce(): pl.pallas_call(reduce_kernel, out_shape=[jax.ShapeDtypeStruct((rows, size...  28.6 us
    dot_general x1, matrix products, expert_backward(): lax.dot_general(cot_rows, w_down, contract_cols, preferred_element_type=j...  8.58 us
    dot_general x1, matrix products, expert_backward(): up_value = jnp.dot(in_rows, w_up, preferred_element_type=jnp.float32)  8.08 us
    dot_general x1, matrix products, expert_backward(): lax.dot_general(in_rows, grad_pre, contract_rows, preferred_element_type=...  7.75 us
    dot_general x1, matrix products, expert_backward(): gate_pre = jnp.dot(in_rows, w_gate, preferred_element_type=jnp.float32)  4.94 us
    dot_general x1, matrix products, expert_backward(): lax.dot_general(in_rows, grad_upval, contract_rows, preferred_element_typ...  4.93 us
    dot_general x1, matrix products, expert_backward(): lax.dot_general(grad_upval, w_up, contract_cols, preferred_element_type=j...  4.83 us

profile of v1, /device:TPU:0, one launch (start us, length us, event | category | flops | bytes accessed | tf_op | source)
XLA Modules:
  0.0 121.5 jit_solution(12264776260941711874)
XLA Ops:
  0.6 0.7 fusion.14
  1.4 0.6 broadcast_in_dim.61.gate
  2.0 39.9 %shard_map.110 = (bf16[4,192,2048]{2,1,0:T(8,128)(2,1)}, bf16[4,192,2048]{2,1,0:T(8,128)(2,1)}, f32[4,8,256]{2,1,0:T(8,128)}) custom-call(bf16[192,2048]{1,0:T(8,128)(2,1)} %tok.1, bf16[192,2048]{1,0:T(8,128)(2,1)} %cot.1, f32[4,8,256]{2,1,0:T(8,128)} %broadcast_in_dim.61.gate), custom_call_target="tpu_custom_call" | custom-call | tf_op jit(solution)/shard_map/pallas_call | solution.py:212
  42.0 0.0 copy-start.2
  42.0 0.0 copy-start.6
  42.0 8.1 %fusion.6 = f32[768,896]{1,0:T(8,128)} fusion(bf16[768,2048]{1,0:T(8,128)(2,1)} %bitcast.55, bf16[1,2048,896]{2,1,0:T(8,128)(2,1)} %param.12), kind=kOutput, calls=%fused_computation.8 | convolution fusion | flops 2818572288 | bytes 9568256 | tf_op jit(solution)/shard_map/dot_general | solution.py:11
  50.1 0.0 copy-done.2
  50.1 0.0 copy-done.6
  50.1 0.0 copy-start.5
  50.1 4.9 %fusion.2 = f32[768,896]{1,0:T(8,128)} fusion(bf16[768,2048]{1,0:T(8,128)(2,1)S(1)} %bitcast.57, bf16[1,2048,896]{2,1,0:T(8,128)(2,1)S(1)} %copy-done.2), kind=kOutput, calls=%fused_computation.4 | convolution fusion | flops 2818572288 | bytes 9568256 | tf_op jit(solution)/shard_map/dot_general | solution.py:10
  55.0 0.8 slice_reduce_fusion
  55.8 0.1 mul.42
  55.9 0.0 copy-done.5
  55.9 0.0 copy-start.3
  55.9 8.6 %multiply_reduce_fusion = (f32[768]{0:T(1024)S(1)}, bf16[768,896]{1,0:T(8,128)(2,1)}, bf16[768,896]{1,0:T(8,128)(2,1)S(1)}, bf16[768,896]{1,0:T(8,128)(2,1)S(1)}) fusion(f32[768,896]{1,0:T(8,128)} %fusion.6, f32[768,896]{1,0:T(8,128)} %fusion.2, f32[768]{0:T(1024)S(1)} %mul.42, bf16[768,2048]{1,0:T(8,128)(2,1)S(1)} %bitcast.53, bf16[1,896,2048]{2,1,0:T(8,128)(2,1)} %param.13), kind=kOutput, calls=%fused_computation.16 | convolution fusion | flops 2831645952 | bytes 16455680 | tf_op jit(solution)/shard_map/dot_general | solution.py:17
  64.5 0.0 copy-start.8
  64.5 0.0 copy-start.9
  64.5 0.0 copy-done.3
  64.5 0.0 copy-start.4
  64.5 3.4 %fusion = f32[768,2048]{1,0:T(8,128)S(1)} fusion(bf16[768,896]{1,0:T(8,128)(2,1)S(1)} %get-tuple-element.21, bf16[1,2048,896]{2,1,0:T(8,128)(2,1)S(1)} %copy-done.3), kind=kOutput, calls=%fused_computation.2 | convolution fusion | flops 2818572288 | bytes 11337728 | tf_op jit(solution)/shard_map/dot_general | solution.py:36
  67.9 0.0 copy-done.8
  67.9 0.0 copy-done.9
  67.9 0.0 copy-done.4
  68.0 4.8 %add_convert_fusion = bf16[768,2048]{1,0:T(8,128)(2,1)} fusion(f32[768,2048]{1,0:T(8,128)S(1)} %fusion, bf16[768,896]{1,0:T(8,128)(2,1)S(1)} %get-tuple-element.22, bf16[1,2048,896]{2,1,0:T(8,128)(2,1)S(1)} %copy-done.4), kind=kOutput, calls=%fused_computation.1 | convolution fusion | flops 2821718016 | bytes 14483456 | tf_op jit(solution)/shard_map/dot_general | solution.py:37
  72.8 0.0 copy-start.1
  72.8 0.1 reshape.32
  72.9 0.6 broadcast_in_dim.62.gate
  73.5 28.6 %shard_map.111 = (bf16[192,256]{1,0:T(8,128)(2,1)}, f32[4,8,256]{2,1,0:T(8,128)}) custom-call(bf16[4,192,2048]{2,1,0:T(8,128)(2,1)} %bitcast.44, f32[4,8,256]{2,1,0:T(8,128)} %broadcast_in_dim.62.gate), custom_call_target="tpu_custom_call" | custom-call | tf_op jit(solution)/shard_map/pallas_call | solution.py:284
  102.1 0.8 fusion.18
  102.9 0.0 copy-done.1
  102.9 0.6 select_select_fusion
  103.4 0.0 copy-start.7
  103.4 0.0 copy-start.10
  103.4 7.7 %convert_bitcast_fusion.2 = bf16[1,2048,896]{2,1,0:T(8,128)(2,1)} fusion(bf16[768,2048]{1,0:T(8,128)(2,1)} %bitcast.56, bf16[768,896]{1,0:T(8,128)(2,1)} %copy-done.8), kind=kOutput, calls=%fused_computation.14 | convolution fusion | flops 2820407296 | bytes 8192000 | tf_op jit(solution)/shard_map/dot_general | solution.py:30
  111.2 0.0 copy-done.7
  111.2 0.0 copy-done.10
  111.2 0.0 copy-start.11
  111.2 4.9 %convert_bitcast_fusion.1 = bf16[1,2048,896]{2,1,0:T(8,128)(2,1)} fusion(bf16[768,2048]{1,0:T(8,128)(2,1)S(1)} %bitcast.58, bf16[768,896]{1,0:T(8,128)(2,1)S(1)} %copy-done.10), kind=kOutput, calls=%fused_computation.13 | convolution fusion | flops 2820407296 | bytes 8192000 | tf_op jit(solution)/shard_map/dot_general | solution.py:33
  116.1 0.0 copy-done.11
  116.1 0.0 copy-start
  116.1 4.7 %convert_bitcast_fusion = bf16[1,896,2048]{2,1,0:T(8,128)(2,1)} fusion(bf16[768,896]{1,0:T(8,128)(2,1)S(1)} %copy-done.11, bf16[768,2048]{1,0:T(8,128)(2,1)S(1)} %bitcast.54, f32[768]{0:T(1024)S(1)} %mul.42), kind=kOutput, calls=%fused_computation.12 | convolution fusion | flops 2825125888 | bytes 8195072 | tf_op jit(solution)/shard_map/dot_general | solution.py:27
  120.8 0.0 copy-done
  120.8 0.6 copy.13
  (2 shorter events, 0.0 us)
Async XLA Ops:
  42.0 8.1 %copy-start.2 = (bf16[1,2048,896]{2,1,0:T(8,128)(2,1)S(1)}, bf16[1,2048,896]{2,1,0:T(8,128)(2,1)}, u32[]{:S(2)}) copy-start(bf16[1,2048,896]{2,1,0:T(8,128)(2,1)} %param.11) | copy-start | bytes 11010052
  42.0 8.1 %copy-start.6 = (bf16[4,192,2048]{2,1,0:T(8,128)(2,1)S(1)}, bf16[4,192,2048]{2,1,0:T(8,128)(2,1)}, u32[]{:S(2)}) copy-start(bf16[4,192,2048]{2,1,0:T(8,128)(2,1)} %get-tuple-element.12) | copy-start | bytes 9437188
  50.1 5.8 %copy-start.5 = (bf16[4,192,2048]{2,1,0:T(8,128)(2,1)S(1)}, bf16[4,192,2048]{2,1,0:T(8,128)(2,1)}, u32[]{:S(2)}) copy-start(bf16[4,192,2048]{2,1,0:T(8,128)(2,1)} %get-tuple-element.11) | copy-start | bytes 9437188
  55.9 8.6 %copy-start.3 = (bf16[1,2048,896]{2,1,0:T(8,128)(2,1)S(1)}, bf16[1,2048,896]{2,1,0:T(8,128)(2,1)}, u32[]{:S(2)}) copy-start(bf16[1,2048,896]{2,1,0:T(8,128)(2,1)} %param.11) | copy-start | bytes 11010052
  64.5 3.5 %copy-start.8 = (bf16[768,896]{1,0:T(8,128)(2,1)}, bf16[768,896]{1,0:T(8,128)(2,1)S(1)}, u32[]{:S(2)}) copy-start(bf16[768,896]{1,0:T(8,128)(2,1)S(1)} %get-tuple-element.21) | copy-start | bytes 4128772
  64.5 3.5 %copy-start.9 = (bf16[768,896]{1,0:T(8,128)(2,1)}, bf16[768,896]{1,0:T(8,128)(2,1)S(1)}, u32[]{:S(2)}) copy-start(bf16[768,896]{1,0:T(8,128)(2,1)S(1)} %get-tuple-element.22) | copy-start | bytes 4128772
  64.5 3.5 %copy-start.4 = (bf16[1,2048,896]{2,1,0:T(8,128)(2,1)S(1)}, bf16[1,2048,896]{2,1,0:T(8,128)(2,1)}, u32[]{:S(2)}) copy-start(bf16[1,2048,896]{2,1,0:T(8,128)(2,1)} %param.12) | copy-start | bytes 11010052
  72.8 30.1 %copy-start.1 = (s32[192,2]{0,1:T(2,128)S(1)}, s32[192,2]{0,1:T(2,128)}, u32[]{:S(2)}) copy-start(s32[192,2]{0,1:T(2,128)} %param.9) | copy-start | bytes 4612
  103.4 7.8 %copy-start.7 = (bf16[4,192,2048]{2,1,0:T(8,128)(2,1)S(1)}, bf16[4,192,2048]{2,1,0:T(8,128)(2,1)}, u32[]{:S(2)}) copy-start(bf16[4,192,2048]{2,1,0:T(8,128)(2,1)} %get-tuple-element.12) | copy-start | bytes 9437188
  103.4 7.8 %copy-start.10 = (bf16[768,896]{1,0:T(8,128)(2,1)S(1)}, bf16[768,896]{1,0:T(8,128)(2,1)}, u32[]{:S(2)}) copy-start(bf16[768,896]{1,0:T(8,128)(2,1)} %copy-done.9) | copy-start | bytes 4128772
  111.2 4.9 %copy-start.11 = (bf16[768,896]{1,0:T(8,128)(2,1)S(1)}, bf16[768,896]{1,0:T(8,128)(2,1)}, u32[]{:S(2)}) copy-start(bf16[768,896]{1,0:T(8,128)(2,1)} %get-tuple-element.20) | copy-start | bytes 4128772
  116.1 4.7 %copy-start = (bf16[192,256]{1,0:T(8,128)(2,1)S(1)}, bf16[192,256]{1,0:T(8,128)(2,1)}, u32[]{:S(2)}) copy-start(bf16[192,256]{1,0:T(8,128)(2,1)} %get-tuple-element.32) | copy-start | bytes 294916

commit v2 on v1

--- a/solution.py
+++ b/solution.py
@@ -165,9 +165,7 @@
         return pl.ds(pl.multiple_of(start, 128), size)
 
     low, high = cols(quarter * q, eighth), cols(quarter * q + eighth, eighth)
-    full = cols(quarter * q, quarter)
     far_low, far_high = cols(quarter * far, eighth), cols(quarter * far + eighth, eighth)
-    far_full = cols(quarter * far, quarter)
     pairs = ((tok, tok_out), (cot, cot_out))
     own = [
         pltpu.make_async_copy(src, dst.at[0], own_sem.at[a]) for a, (src, dst) in enumerate(pairs)
@@ -178,12 +176,12 @@
     gates = [do.send(gate.at[j], gate_out.at[j], flip(me, j), t) for j in (1, 2, 3)]
     relayed, direct = [], []
     for src, dst in pairs:
-        for j, where in ((3, full), (1, high), (2, high)):
-            copy = do.send(src.at[:, where], dst.at[j, :, where], flip(me, j), t)
-            relayed.append((copy, dst, j, where))
+        for j in (3, 1, 2):
+            copy = do.send(src.at[:, high], dst.at[j, :, high], flip(me, j), t)
+            relayed.append((copy, dst, j, high))
     for src, dst in pairs:
         for where in (low, far_low):
-            for j in (1, 2):
+            for j in (3, 1, 2):
                 copy = do.send(src.at[:, where], dst.at[j, :, where], flip(me, j), t)
                 direct.append((copy, dst, j, where))
     last = []
@@ -191,7 +189,7 @@
         copy.wait_recv()
         piece = dst.at[j, :, where]
         moved = do.send(piece, piece, me, flip(t, 2))
-        direct.append((moved, dst, j, far_full if j == 3 else far_high))
+        direct.append((moved, dst, j, far_high))
         last.append(do.send(piece, piece, me, flip(t, 1)))
     for copy, dst, j, where in direct:
         copy.wait_recv()
@@ -215,8 +213,8 @@
         in_specs=[vmem] * 3,
         out_specs=[vmem] * 3,
         scratch_shapes=[
-            pltpu.SemaphoreType.DMA((43,)),
-            pltpu.SemaphoreType.DMA((43,)),
+            pltpu.SemaphoreType.DMA((51,)),
+            pltpu.SemaphoreType.DMA((51,)),
             pltpu.SemaphoreType.DMA((2,)),
         ],
         compiler_params=pltpu.CompilerParams(has_side_effects=True),

time: 122 us -> 126 us (1.033)
  Pallas kernels: 68.6 us -> 72.8 us
    pallas_call x1, Pallas kernels: 39.9 us -> 42.7 us  [gather(): pl.pallas_call(gather_kernel, out_shape=[shape, shape, jax.ShapeDtypeStru...]
    pallas_call x1, Pallas kernels: 28.6 us -> 30.1 us  [reduce(): pl.pallas_call(reduce_kernel, out_shape=[jax.ShapeDtypeStruct((rows, size...]
where the time goes in v2:
time: 126 us
  Pallas kernels  72.8 us (58%)
  matrix products  47.2 us (37%)
  local copies, waits for them, and re-layouts  3.62 us (3%)
  other arithmetic  1.32 us (1%)
    pallas_call x1, Pallas kernels, gather(): pl.pallas_call(gather_kernel, out_shape=[shape, shape, jax.ShapeDtypeStru...  42.7 us
    pallas_call x1, Pallas kernels, reduce(): pl.pallas_call(reduce_kernel, out_shape=[jax.ShapeDtypeStruct((rows, size...  30.1 us
    dot_general x1, matrix products, expert_backward(): lax.dot_general(cot_rows, w_down, contract_cols, preferred_element_type=j...  8.58 us
    dot_general x1, matrix products, expert_backward(): up_value = jnp.dot(in_rows, w_up, preferred_element_type=jnp.float32)  8.07 us
    dot_general x1, matrix products, expert_backward(): lax.dot_general(in_rows, grad_pre, contract_rows, preferred_element_type=...  7.75 us
    dot_general x1, matrix products, expert_backward(): gate_pre = jnp.dot(in_rows, w_gate, preferred_element_type=jnp.float32)  4.94 us
    dot_general x1, matrix products, expert_backward(): lax.dot_general(in_rows, grad_upval, contract_rows, preferred_element_typ...  4.93 us
    dot_general x1, matrix products, expert_backward(): lax.dot_general(grad_upval, w_up, contract_cols, preferred_element_type=j...  4.83 us

profile of v2, /device:TPU:0, one launch (start us, length us, event | category | flops | bytes accessed | tf_op | source)
XLA Modules:
  0.0 125.7 jit_solution(9616425183656859252)
XLA Ops:
  0.6 0.7 fusion.14
  1.4 0.6 broadcast_in_dim.61.gate
  2.0 42.7 %shard_map.110 = (bf16[4,192,2048]{2,1,0:T(8,128)(2,1)}, bf16[4,192,2048]{2,1,0:T(8,128)(2,1)}, f32[4,8,256]{2,1,0:T(8,128)}) custom-call(bf16[192,2048]{1,0:T(8,128)(2,1)} %tok.1, bf16[192,2048]{1,0:T(8,128)(2,1)} %cot.1, f32[4,8,256]{2,1,0:T(8,128)} %broadcast_in_dim.61.gate), custom_call_target="tpu_custom_call" | custom-call | tf_op jit(solution)/shard_map/pallas_call | solution.py:210
  44.7 0.0 copy-start.2
  44.7 0.0 copy-start.6
  44.7 8.1 %fusion.6 = f32[768,896]{1,0:T(8,128)} fusion(bf16[768,2048]{1,0:T(8,128)(2,1)} %bitcast.55, bf16[1,2048,896]{2,1,0:T(8,128)(2,1)} %param.12), kind=kOutput, calls=%fused_computation.8 | convolution fusion | flops 2818572288 | bytes 9568256 | tf_op jit(solution)/shard_map/dot_general | solution.py:11
  52.8 0.0 copy-done.2
  52.8 0.0 copy-done.6
  52.8 0.0 copy-start.5
  52.8 4.9 %fusion.2 = f32[768,896]{1,0:T(8,128)} fusion(bf16[768,2048]{1,0:T(8,128)(2,1)S(1)} %bitcast.57, bf16[1,2048,896]{2,1,0:T(8,128)(2,1)S(1)} %copy-done.2), kind=kOutput, calls=%fused_computation.4 | convolution fusion | flops 2818572288 | bytes 9568256 | tf_op jit(solution)/shard_map/dot_general | solution.py:10
  57.8 0.8 slice_reduce_fusion
  58.5 0.1 mul.42
  58.6 0.0 copy-done.5
  58.6 0.0 copy-start.3
  58.6 8.6 %multiply_reduce_fusion = (f32[768]{0:T(1024)S(1)}, bf16[768,896]{1,0:T(8,128)(2,1)}, bf16[768,896]{1,0:T(8,128)(2,1)S(1)}, bf16[768,896]{1,0:T(8,128)(2,1)S(1)}) fusion(f32[768,896]{1,0:T(8,128)} %fusion.6, f32[768,896]{1,0:T(8,128)} %fusion.2, f32[768]{0:T(1024)S(1)} %mul.42, bf16[768,2048]{1,0:T(8,128)(2,1)S(1)} %bitcast.53, bf16[1,896,2048]{2,1,0:T(8,128)(2,1)} %param.13), kind=kOutput, calls=%fused_computation.16 | convolution fusion | flops 2831645952 | bytes 16455680 | tf_op jit(solution)/shard_map/dot_general | solution.py:17
  67.2 0.0 copy-start.8
  67.2 0.0 copy-start.9
  67.2 0.0 copy-done.3
  67.2 0.0 copy-start.4
  67.2 3.4 %fusion = f32[768,2048]{1,0:T(8,128)S(1)} fusion(bf16[768,896]{1,0:T(8,128)(2,1)S(1)} %get-tuple-element.21, bf16[1,2048,896]{2,1,0:T(8,128)(2,1)S(1)} %copy-done.3), kind=kOutput, calls=%fused_computation.2 | convolution fusion | flops 2818572288 | bytes 11337728 | tf_op jit(solution)/shard_map/dot_general | solution.py:36
  70.7 0.0 copy-done.8
  70.7 0.0 copy-done.9
  70.7 0.0 copy-done.4
  70.7 4.8 %add_convert_fusion = bf16[768,2048]{1,0:T(8,128)(2,1)} fusion(f32[768,2048]{1,0:T(8,128)S(1)} %fusion, bf16[768,896]{1,0:T(8,128)(2,1)S(1)} %get-tuple-element.22, bf16[1,2048,896]{2,1,0:T(8,128)(2,1)S(1)} %copy-done.4), kind=kOutput, calls=%fused_computation.1 | convolution fusion | flops 2821718016 | bytes 14483456 | tf_op jit(solution)/shard_map/dot_general | solution.py:37
  75.5 0.0 copy-start.1
  75.5 0.1 reshape.32
  75.6 0.6 broadcast_in_dim.62.gate
  76.3 30.1 %shard_map.111 = (bf16[192,256]{1,0:T(8,128)(2,1)}, f32[4,8,256]{2,1,0:T(8,128)}) custom-call(bf16[4,192,2048]{2,1,0:T(8,128)(2,1)} %bitcast.44, f32[4,8,256]{2,1,0:T(8,128)} %broadcast_in_dim.62.gate), custom_call_target="tpu_custom_call" | custom-call | tf_op jit(solution)/shard_map/pallas_call | solution.py:282
  106.4 0.8 fusion.18
  107.1 0.0 copy-done.1
  107.1 0.6 select_select_fusion
  107.7 0.0 copy-start.7
  107.7 0.0 copy-start.10
  107.7 7.7 %convert_bitcast_fusion.2 = bf16[1,2048,896]{2,1,0:T(8,128)(2,1)} fusion(bf16[768,2048]{1,0:T(8,128)(2,1)} %bitcast.56, bf16[768,896]{1,0:T(8,128)(2,1)} %copy-done.8), kind=kOutput, calls=%fused_computation.14 | convolution fusion | flops 2820407296 | bytes 8192000 | tf_op jit(solution)/shard_map/dot_general | solution.py:30
  115.5 0.0 copy-done.7
  115.5 0.0 copy-done.10
  115.5 0.0 copy-start.11
  115.5 4.9 %convert_bitcast_fusion.1 = bf16[1,2048,896]{2,1,0:T(8,128)(2,1)} fusion(bf16[768,2048]{1,0:T(8,128)(2,1)S(1)} %bitcast.58, bf16[768,896]{1,0:T(8,128)(2,1)S(1)} %copy-done.10), kind=kOutput, calls=%fused_computation.13 | convolution fusion | flops 2820407296 | bytes 8192000 | tf_op jit(solution)/shard_map/dot_general | solution.py:33
  120.4 0.0 copy-done.11
  120.4 0.0 copy-start
  120.4 4.7 %convert_bitcast_fusion = bf16[1,896,2048]{2,1,0:T(8,128)(2,1)} fusion(bf16[768,896]{1,0:T(8,128)(2,1)S(1)} %copy-done.11, bf16[768,2048]{1,0:T(8,128)(2,1)S(1)} %bitcast.54, f32[768]{0:T(1024)S(1)} %mul.42), kind=kOutput, calls=%fused_computation.12 | convolution fusion | flops 2825125888 | bytes 8195072 | tf_op jit(solution)/shard_map/dot_general | solution.py:27
  125.1 0.0 copy-done
  125.1 0.6 copy.13
  (2 shorter events, 0.0 us)
Async XLA Ops:
  44.7 8.1 %copy-start.2 = (bf16[1,2048,896]{2,1,0:T(8,128)(2,1)S(1)}, bf16[1,2048,896]{2,1,0:T(8,128)(2,1)}, u32[]{:S(2)}) copy-start(bf16[1,2048,896]{2,1,0:T(8,128)(2,1)} %param.11) | copy-start | bytes 11010052
  44.7 8.1 %copy-start.6 = (bf16[4,192,2048]{2,1,0:T(8,128)(2,1)S(1)}, bf16[4,192,2048]{2,1,0:T(8,128)(2,1)}, u32[]{:S(2)}) copy-start(bf16[4,192,2048]{2,1,0:T(8,128)(2,1)} %get-tuple-element.12) | copy-start | bytes 9437188
  52.8 5.8 %copy-start.5 = (bf16[4,192,2048]{2,1,0:T(8,128)(2,1)S(1)}, bf16[4,192,2048]{2,1,0:T(8,128)(2,1)}, u32[]{:S(2)}) copy-start(bf16[4,192,2048]{2,1,0:T(8,128)(2,1)} %get-tuple-element.11) | copy-start | bytes 9437188
  58.6 8.6 %copy-start.3 = (bf16[1,2048,896]{2,1,0:T(8,128)(2,1)S(1)}, bf16[1,2048,896]{2,1,0:T(8,128)(2,1)}, u32[]{:S(2)}) copy-start(bf16[1,2048,896]{2,1,0:T(8,128)(2,1)} %param.11) | copy-start | bytes 11010052
  67.2 3.5 %copy-start.8 = (bf16[768,896]{1,0:T(8,128)(2,1)}, bf16[768,896]{1,0:T(8,128)(2,1)S(1)}, u32[]{:S(2)}) copy-start(bf16[768,896]{1,0:T(8,128)(2,1)S(1)} %get-tuple-element.21) | copy-start | bytes 4128772
  67.2 3.5 %copy-start.9 = (bf16[768,896]{1,0:T(8,128)(2,1)}, bf16[768,896]{1,0:T(8,128)(2,1)S(1)}, u32[]{:S(2)}) copy-start(bf16[768,896]{1,0:T(8,128)(2,1)S(1)} %get-tuple-element.22) | copy-start | bytes 4128772
  67.2 3.5 %copy-start.4 = (bf16[1,2048,896]{2,1,0:T(8,128)(2,1)S(1)}, bf16[1,2048,896]{2,1,0:T(8,128)(2,1)}, u32[]{:S(2)}) copy-start(bf16[1,2048,896]{2,1,0:T(8,128)(2,1)} %param.12) | copy-start | bytes 11010052
  75.5 31.6 %copy-start.1 = (s32[192,2]{0,1:T(2,128)S(1)}, s32[192,2]{0,1:T(2,128)}, u32[]{:S(2)}) copy-start(s32[192,2]{0,1:T(2,128)} %param.9) | copy-start | bytes 4612
  107.7 7.8 %copy-start.7 = (bf16[4,192,2048]{2,1,0:T(8,128)(2,1)S(1)}, bf16[4,192,2048]{2,1,0:T(8,128)(2,1)}, u32[]{:S(2)}) copy-start(bf16[4,192,2048]{2,1,0:T(8,128)(2,1)} %get-tuple-element.12) | copy-start | bytes 9437188
  107.7 7.8 %copy-start.10 = (bf16[768,896]{1,0:T(8,128)(2,1)S(1)}, bf16[768,896]{1,0:T(8,128)(2,1)}, u32[]{:S(2)}) copy-start(bf16[768,896]{1,0:T(8,128)(2,1)} %copy-done.9) | copy-start | bytes 4128772
  115.5 4.9 %copy-start.11 = (bf16[768,896]{1,0:T(8,128)(2,1)S(1)}, bf16[768,896]{1,0:T(8,128)(2,1)}, u32[]{:S(2)}) copy-start(bf16[768,896]{1,0:T(8,128)(2,1)} %get-tuple-element.20) | copy-start | bytes 4128772
  120.4 4.7 %copy-start = (bf16[192,256]{1,0:T(8,128)(2,1)S(1)}, bf16[192,256]{1,0:T(8,128)(2,1)}, u32[]{:S(2)}) copy-start(bf16[192,256]{1,0:T(8,128)(2,1)} %get-tuple-element.32) | copy-start | bytes 294916

commit v3 on v1

--- a/solution.py
+++ b/solution.py
@@ -219,7 +219,7 @@
             pltpu.SemaphoreType.DMA((43,)),
             pltpu.SemaphoreType.DMA((2,)),
         ],
-        compiler_params=pltpu.CompilerParams(has_side_effects=True),
+        compiler_params=pltpu.CompilerParams(has_side_effects=True, vmem_limit_bytes=14 << 20),
     )(tokens, cotangent, gate)
 
 
@@ -300,7 +300,7 @@
             pltpu.SemaphoreType.DMA((37,)),
             pltpu.SemaphoreType.DMA((37,)),
         ],
-        compiler_params=pltpu.CompilerParams(has_side_effects=True),
+        compiler_params=pltpu.CompilerParams(has_side_effects=True, vmem_limit_bytes=20 << 20),
     )(part, gate)
 
 

time: 122 us -> 114 us (0.934)
  Pallas kernels: 68.6 us -> 62.1 us
  matrix products: 47.2 us -> 45.9 us
    pallas_call x1, Pallas kernels: 39.9 us -> 36 us  [gather(): pl.pallas_call(gather_kernel, out_shape=[shape, shape, jax.ShapeDtypeStru...]
    pallas_call x1, Pallas kernels: 28.6 us -> 26.1 us  [reduce(): pl.pallas_call(reduce_kernel, out_shape=[jax.ShapeDtypeStruct((rows, size...]
    unnamed x25 -> x29, local copies, waits for them, and re-layouts: 0.69 us -> 2.96 us
    dot_general x1, matrix products: 7.75 us -> 6.36 us  [expert_backward(): lax.dot_general(in_rows, grad_pre, contract_rows, preferred_element_type=...]
    broadcast_in_dim x2, local copies, waits for them, and re-layouts: 1.24 us -> 0.01 us  [tiles(): jnp.broadcast_to(padded[:, None, :], (padded.shape[0], 8, padded.shape[1]))]
where the time goes in v3:
time: 114 us; the launch traced here: 113 us
  Pallas kernels  62.1 us (54%)
  matrix products  45.9 us (40%)
  local copies, waits for them, and re-layouts  3.16 us (3%)
  other arithmetic  1.33 us (1%)
    pallas_call x1, Pallas kernels, gather(): pl.pallas_call(gather_kernel, out_shape=[shape, shape, jax.ShapeDtypeStru...  36 us
    pallas_call x1, Pallas kernels, reduce(): pl.pallas_call(reduce_kernel, out_shape=[jax.ShapeDtypeStruct((rows, size...  26.1 us
    dot_general x1, matrix products, expert_backward(): up_value = jnp.dot(in_rows, w_up, preferred_element_type=jnp.float32)  9.28 us
    dot_general x1, matrix products, expert_backward(): lax.dot_general(cot_rows, w_down, contract_cols, preferred_element_type=j...  8.58 us
    dot_general x1, matrix products, expert_backward(): lax.dot_general(in_rows, grad_pre, contract_rows, preferred_element_type=...  6.36 us
    dot_general x1, matrix products, expert_backward(): lax.dot_general(in_rows, grad_upval, contract_rows, preferred_element_typ...  4.97 us
    dot_general x1, matrix products, expert_backward(): gate_pre = jnp.dot(in_rows, w_gate, preferred_element_type=jnp.float32)  4.94 us
    dot_general x1, matrix products, expert_backward(): lax.dot_general(hidden, scaled_cot, contract_rows, preferred_element_type...  4.66 us

profile of v3, /device:TPU:0, one launch (start us, length us, event | category | flops | bytes accessed | tf_op | source)
XLA Modules:
  0.0 113.3 jit_solution(5648277116402617579)
XLA Ops:
  0.6 0.7 fusion.14
  1.4 0.0 copy-start
  1.4 1.1 copy-done
  2.5 0.0 copy-start.1
  2.5 1.1 copy-done.1
  3.7 36.0 %shard_map.110 = (bf16[4,192,2048]{2,1,0:T(8,128)(2,1)S(1)}, bf16[4,192,2048]{2,1,0:T(8,128)(2,1)S(1)}, f32[4,8,256]{2,1,0:T(8,128)S(1)}) custom-call(bf16[192,2048]{1,0:T(8,128)(2,1)S(1)} %copy-done, bf16[192,2048]{1,0:T(8,128)(2,1)S(1)} %copy-done.1, f32[4,8,256]{2,1,0:T(8,128)S(1)} %broadcast_in_dim.61.gate), custom_call_target="tpu_custom_call" | custom-call | tf_op jit(solution)/shard_map/pallas_call | solution.py:212
  39.6 0.0 copy-start.4
  39.7 0.0 copy-start.2
  39.7 0.0 copy-start.7
  39.7 9.3 %fusion.6 = f32[768,896]{1,0:T(8,128)} fusion(bf16[768,2048]{1,0:T(8,128)(2,1)S(1)} %bitcast.47, bf16[1,2048,896]{2,1,0:T(8,128)(2,1)} %param.12), kind=kOutput, calls=%fused_computation.8 | convolution fusion | flops 2818572288 | bytes 9568256 | tf_op jit(solution)/shard_map/dot_general | solution.py:11
  49.0 0.0 copy-done.4
  49.0 0.0 copy-done.7
  49.0 4.9 %fusion.2 = f32[768,896]{1,0:T(8,128)} fusion(bf16[768,2048]{1,0:T(8,128)(2,1)S(1)} %bitcast.48, bf16[1,2048,896]{2,1,0:T(8,128)(2,1)S(1)} %copy-done.7), kind=kOutput, calls=%fused_computation.4 | convolution fusion | flops 2818572288 | bytes 9568256 | tf_op jit(solution)/shard_map/dot_general | solution.py:10
  53.9 0.1 mul.42
  54.0 0.0 copy-done.2
  54.0 0.0 copy-start.8
  54.0 8.6 %multiply_reduce_fusion = (f32[768]{0:T(1024)S(1)}, bf16[768,896]{1,0:T(8,128)(2,1)}, bf16[768,896]{1,0:T(8,128)(2,1)S(1)}, bf16[768,896]{1,0:T(8,128)(2,1)S(1)}) fusion(f32[768,896]{1,0:T(8,128)} %fusion.6, f32[768,896]{1,0:T(8,128)} %fusion.2, f32[768]{0:T(1024)S(1)} %mul.42, bf16[768,2048]{1,0:T(8,128)(2,1)S(1)} %bitcast.45, bf16[1,896,2048]{2,1,0:T(8,128)(2,1)} %param.13), kind=kOutput, calls=%fused_computation.16 | convolution fusion | flops 2831645952 | bytes 16455680 | tf_op jit(solution)/shard_map/dot_general | solution.py:17
  62.6 0.0 copy-start.11
  62.6 0.0 copy-start.10
  62.6 0.0 copy-done.8
  62.6 0.0 copy-start.9
  62.6 3.4 %fusion = f32[768,2048]{1,0:T(8,128)S(1)} fusion(bf16[768,896]{1,0:T(8,128)(2,1)S(1)} %get-tuple-element.21, bf16[1,2048,896]{2,1,0:T(8,128)(2,1)S(1)} %copy-done.8), kind=kOutput, calls=%fused_computation.2 | convolution fusion | flops 2818572288 | bytes 11337728 | tf_op jit(solution)/shard_map/dot_general | solution.py:36
  66.1 0.0 copy-done.11
  66.1 0.0 copy-done.9
  66.1 3.7 %add_convert_fusion = bf16[768,2048]{1,0:T(8,128)(2,1)S(1)} fusion(f32[768,2048]{1,0:T(8,128)S(1)} %fusion, bf16[768,896]{1,0:T(8,128)(2,1)S(1)} %get-tuple-element.22, bf16[1,2048,896]{2,1,0:T(8,128)(2,1)S(1)} %copy-done.9), kind=kOutput, calls=%fused_computation.1 | convolution fusion | flops 2821718016 | bytes 14483456 | tf_op jit(solution)/shard_map/dot_general | solution.py:37
  69.8 0.0 copy-done.10
  69.8 0.0 copy-start.6
  69.8 0.1 reshape.32
  69.9 0.0 copy-start.5
  69.9 26.1 %shard_map.111 = (bf16[192,256]{1,0:T(8,128)(2,1)S(1)}, f32[4,8,256]{2,1,0:T(8,128)S(1)}) custom-call(bf16[4,192,2048]{2,1,0:T(8,128)(2,1)S(1)} %bitcast.44, f32[4,8,256]{2,1,0:T(8,128)S(1)} %broadcast_in_dim.62.gate), custom_call_target="tpu_custom_call" | custom-call | tf_op jit(solution)/shard_map/pallas_call | solution.py:284
  96.0 0.0 copy-done.6
  96.0 0.6 select_select_fusion
  96.6 0.0 copy-done.5
  96.6 0.0 copy-start.12
  96.6 6.4 %convert_bitcast_fusion.2 = bf16[1,2048,896]{2,1,0:T(8,128)(2,1)} fusion(bf16[768,2048]{1,0:T(8,128)(2,1)S(1)} %bitcast.49, bf16[768,896]{1,0:T(8,128)(2,1)} %copy-done.10), kind=kOutput, calls=%fused_computation.14 | convolution fusion | flops 2820407296 | bytes 8192000 | tf_op jit(solution)/shard_map/dot_general | solution.py:30
  103.0 0.0 copy-done.12
  103.0 0.0 copy-start.3
  103.0 0.0 copy-start.13
  103.0 5.0 %convert_bitcast_fusion.1 = bf16[1,2048,896]{2,1,0:T(8,128)(2,1)} fusion(bf16[768,2048]{1,0:T(8,128)(2,1)S(1)} %bitcast.50, bf16[768,896]{1,0:T(8,128)(2,1)S(1)} %copy-done.12), kind=kOutput, calls=%fused_computation.13 | convolution fusion | flops 2820407296 | bytes 8192000 | tf_op jit(solution)/shard_map/dot_general | solution.py:33
  108.0 0.0 copy-done.3
  108.0 0.0 copy-done.13
  108.0 4.7 %convert_bitcast_fusion = bf16[1,896,2048]{2,1,0:T(8,128)(2,1)} fusion(bf16[768,896]{1,0:T(8,128)(2,1)S(1)} %copy-done.13, bf16[768,2048]{1,0:T(8,128)(2,1)S(1)} %bitcast.46, f32[768]{0:T(1024)S(1)} %mul.42), kind=kOutput, calls=%fused_computation.12 | convolution fusion | flops 2825125888 | bytes 8195072 | tf_op jit(solution)/shard_map/dot_general | solution.py:27
  112.6 0.6 copy.13
  (6 shorter events, 0.1 us)
Async XLA Ops:
  1.4 1.1 %copy-start = (bf16[192,2048]{1,0:T(8,128)(2,1)S(1)}, bf16[192,2048]{1,0:T(8,128)(2,1)}, u32[]{:S(2)}) copy-start(bf16[192,2048]{1,0:T(8,128)(2,1)} %tok.1) | copy-start | bytes 2359300
  2.5 1.1 %copy-start.1 = (bf16[192,2048]{1,0:T(8,128)(2,1)S(1)}, bf16[192,2048]{1,0:T(8,128)(2,1)}, u32[]{:S(2)}) copy-start(bf16[192,2048]{1,0:T(8,128)(2,1)} %cot.1) | copy-start | bytes 2359300
  39.6 9.3 %copy-start.4 = (bf16[4,192,2048]{2,1,0:T(8,128)(2,1)}, bf16[4,192,2048]{2,1,0:T(8,128)(2,1)S(1)}, u32[]{:S(2)}) copy-start(bf16[4,192,2048]{2,1,0:T(8,128)(2,1)S(1)} %get-tuple-element.12) | copy-start | bytes 9437188
  39.7 14.4 %copy-start.2 = (bf16[4,192,2048]{2,1,0:T(8,128)(2,1)}, bf16[4,192,2048]{2,1,0:T(8,128)(2,1)S(1)}, u32[]{:S(2)}) copy-start(bf16[4,192,2048]{2,1,0:T(8,128)(2,1)S(1)} %get-tuple-element.11) | copy-start | bytes 9437188
  39.7 9.3 %copy-start.7 = (bf16[1,2048,896]{2,1,0:T(8,128)(2,1)S(1)}, bf16[1,2048,896]{2,1,0:T(8,128)(2,1)}, u32[]{:S(2)}) copy-start(bf16[1,2048,896]{2,1,0:T(8,128)(2,1)} %param.11) | copy-start | bytes 11010052
  54.0 8.6 %copy-start.8 = (bf16[1,2048,896]{2,1,0:T(8,128)(2,1)S(1)}, bf16[1,2048,896]{2,1,0:T(8,128)(2,1)}, u32[]{:S(2)}) copy-start(bf16[1,2048,896]{2,1,0:T(8,128)(2,1)} %param.11) | copy-start | bytes 11010052
  62.6 3.5 %copy-start.11 = (bf16[768,896]{1,0:T(8,128)(2,1)}, bf16[768,896]{1,0:T(8,128)(2,1)S(1)}, u32[]{:S(2)}) copy-start(bf16[768,896]{1,0:T(8,128)(2,1)S(1)} %get-tuple-element.22) | copy-start | bytes 4128772
  62.6 7.2 %copy-start.10 = (bf16[768,896]{1,0:T(8,128)(2,1)}, bf16[768,896]{1,0:T(8,128)(2,1)S(1)}, u32[]{:S(2)}) copy-start(bf16[768,896]{1,0:T(8,128)(2,1)S(1)} %get-tuple-element.21) | copy-start | bytes 4128772
  62.6 3.5 %copy-start.9 = (bf16[1,2048,896]{2,1,0:T(8,128)(2,1)S(1)}, bf16[1,2048,896]{2,1,0:T(8,128)(2,1)}, u32[]{:S(2)}) copy-start(bf16[1,2048,896]{2,1,0:T(8,128)(2,1)} %param.12) | copy-start | bytes 11010052
  69.8 26.2 %copy-start.6 = (s32[192,2]{0,1:T(2,128)S(1)}, s32[192,2]{0,1:T(2,128)}, u32[]{:S(2)}) copy-start(s32[192,2]{0,1:T(2,128)} %param.9) | copy-start | bytes 4612
  69.9 26.7 %copy-start.5 = (bf16[4,192,2048]{2,1,0:T(8,128)(2,1)S(1)}, bf16[4,192,2048]{2,1,0:T(8,128)(2,1)}, u32[]{:S(2)}) copy-start(bf16[4,192,2048]{2,1,0:T(8,128)(2,1)} %copy-done.4) | copy-start | bytes 9437188
  96.6 6.4 %copy-start.12 = (bf16[768,896]{1,0:T(8,128)(2,1)S(1)}, bf16[768,896]{1,0:T(8,128)(2,1)}, u32[]{:S(2)}) copy-start(bf16[768,896]{1,0:T(8,128)(2,1)} %copy-done.11) | copy-start | bytes 4128772
  103.0 5.0 %copy-start.3 = (bf16[4,192,2048]{2,1,0:T(8,128)(2,1)S(1)}, bf16[4,192,2048]{2,1,0:T(8,128)(2,1)}, u32[]{:S(2)}) copy-start(bf16[4,192,2048]{2,1,0:T(8,128)(2,1)} %copy-done.2) | copy-start | bytes 9437188
  103.0 5.0 %copy-start.13 = (bf16[768,896]{1,0:T(8,128)(2,1)S(1)}, bf16[768,896]{1,0:T(8,128)(2,1)}, u32[]{:S(2)}) copy-start(bf16[768,896]{1,0:T(8,128)(2,1)} %get-tuple-element.20) | copy-start | bytes 4128772
